TPU v7x, 512 devices: a whole 4x4x16 slice. The times are simulated.
512 devices in a mesh: sp: 128 (over z, x, core), tp: 4 (over y).
Axes of the slice: x: 4, y: 4, z: 16, core: 2. Of those that a mesh axis runs over, the one named last changes fastest.
Arguments:
- tokens: bfloat16 [32768, 2048], P(('sp', 'tp')), may hold values from -40 to 40
- w_query: bfloat16 [2048, 1024], P(None, 'tp'), may hold values from -0.125 to 0.125
- w_key: bfloat16 [2048, 256], P(None, 'tp'), may hold values from -0.125 to 0.125
- w_value: bfloat16 [2048, 256], P(None, 'tp'), may hold values from -0.125 to 0.125
- w_out: bfloat16 [1024, 2048], P('tp'), may hold values from -0.1875 to 0.1875
- cum_gate: float32 [16, 32768], P('tp', 'sp'), may hold values from -4684 to 0, as said below
Outputs:
- layer_out: bfloat16 [32768, 2048], P(('sp', 'tp'))
Inputs may be any that keep to these rules, and one draw needn't show every extreme that they name: `cum_gate`: each head's row does not rise along the positions.
All inputs are finite; a program needn't handle non-finite values.
Results may differ from a plain program's by a relative error of at most 0.012.
Values may be sent and summed in bfloat16 or wider, within the bound.
No kernel may reach another device: no remote copies, remote signals or barrier semaphores. Data moves between devices by JAX's collectives and lax.ppermute only.
A program may use at most 64 MiB of HBM per device.

v0:
```python
import math

import jax
import jax.numpy as jnp
from jax import lax
from jax.sharding import PartitionSpec as P

HD = 64


def sent_to_all(x, axis):
    copies = jnp.broadcast_to(x, (lax.axis_size(axis), *x.shape))
    return lax.all_to_all(copies, axis, split_axis=0, concat_axis=0, tiled=True)


def joined_along(parts, dim):
    dims = list(parts.shape[1:])
    dims[dim] *= parts.shape[0]
    return jnp.moveaxis(parts, 0, dim).reshape(dims)


def collect(x, axis, dim):
    parts = sent_to_all(x, axis)
    return joined_along(parts, dim)


def partner(block, axis, bit):
    count = lax.axis_size(axis)
    route = []
    for low in range(count):
        high = low | 1 << bit
        if high != low and high < count:
            route += [(low, high), (high, low)]
    return lax.ppermute(block, axis, route)


def cut_along(x, dim, peers):
    before, after = (x.shape[:dim], x.shape[dim + 1 :])
    return jnp.moveaxis(x.reshape(*before, peers, -1, *after), dim, 0)


def sent_and_summed(x, axis, dim):
    peers = lax.axis_size(axis)
    parts = lax.all_to_all(cut_along(x, dim, peers), axis, 0, 0, tiled=True)
    return jnp.sum(parts.astype(jnp.float32), axis=0)


def per_device(tokens, w_query, w_key, w_value, w_out, cum_gate):
    pieces = collect(tokens, "tp", 0)
    query_part = jnp.dot(pieces, w_query, preferred_element_type=jnp.float32).astype(jnp.bfloat16)
    key_part = jnp.dot(pieces, w_key, preferred_element_type=jnp.float32).astype(jnp.bfloat16)
    value_part = jnp.dot(pieces, w_value, preferred_element_type=jnp.float32).astype(jnp.bfloat16)
    projected = jnp.concatenate([query_part, key_part, value_part], axis=1)
    row_count = projected.shape[0]
    half_rows = row_count // 2
    heads_local = w_query.shape[1] // HD
    kv_local = w_key.shape[1] // HD
    group_size = heads_local // kv_local
    score_factor = float(HD) ** (-0.5)
    query_flat = projected[:, : heads_local * HD]
    key_values = projected[:, heads_local * HD :]
    first_pos = lax.axis_index("sp") * row_count
    own_pos = first_pos + jnp.arange(row_count, dtype=jnp.int32)
    gate_all = lax.all_gather(cum_gate, "sp", axis=1, tiled=True)
    partner_leading = (lax.axis_size("sp") - 1 - lax.axis_index("sp")) * row_count
    moved = query_flat[half_rows:]
    for bit in range(lax.axis_size("sp").bit_length() - 1):
        moved = partner(moved, "sp", bit)
    partner_start = partner_leading + half_rows
    partner_pos = partner_start + jnp.arange(half_rows, dtype=jnp.int32)
    partner_cum = lax.dynamic_slice_in_dim(gate_all, partner_start, half_rows, 1)
    groups = [
        (query_flat[:half_rows], cum_gate[:, :half_rows], own_pos[:half_rows]),
        (moved, partner_cum, partner_pos),
    ]
    prepared = []
    for query_rows, query_gates, query_pos in groups:
        count = query_rows.shape[0]
        prepared.append(
            (
                query_rows.reshape(count, kv_local, group_size, HD),
                query_gates.reshape(kv_local, group_size, count, 1),
                query_pos,
                jnp.max(query_pos),
            )
        )
    initial = tuple(
        (
            (
                jnp.full((kv_local, group_size, member[2].shape[0]), -1e30, jnp.float32),
                jnp.zeros((kv_local, group_size, member[2].shape[0]), jnp.float32),
                jnp.zeros((kv_local, group_size, member[2].shape[0], HD), jnp.float32),
            )
            for member in prepared
        )
    )
    pieces = lax.all_gather(key_values, "sp", axis=0, tiled=True)
    piece_rows = pieces.shape[0]
    key_block = math.gcd(piece_rows, 1024)

    def one_block(index, hidden_vectors):
        block_start = index * key_block
        slab = lax.dynamic_slice_in_dim(pieces, block_start, key_block, 0)
        key_rows = slab[:, : kv_local * HD].reshape(key_block, kv_local, HD)
        value_rows = slab[:, kv_local * HD :].reshape(key_block, kv_local, HD)
        key_cum = lax.dynamic_slice_in_dim(gate_all, block_start, key_block, 1)
        key_cum = key_cum.reshape(kv_local, group_size, 1, key_block)
        key_pos = block_start + jnp.arange(key_block, dtype=jnp.int32)
        results = []
        for member, state in zip(prepared, hidden_vectors):
            queries, query_cum, query_pos, last_pos = member

            def compute(inner, queries=queries, query_cum=query_cum, query_pos=query_pos):
                top_score, weight_sum, accumulated = inner
                scores = (
                    jnp.einsum(
                        "tkgd,skd->kgts", queries, key_rows, preferred_element_type=jnp.float32
                    )
                    * score_factor
                )
                scores = scores + (query_cum - key_cum)
                scores = jnp.where(key_pos[None, :] <= query_pos[:, None], scores, -jnp.inf)
                new_top = jnp.maximum(top_score, jnp.max(scores, axis=-1))
                weights = jnp.exp(scores - new_top[..., None])
                decay = jnp.exp(top_score - new_top)
                weight_sum = weight_sum * decay + jnp.sum(weights, axis=-1)
                update = jnp.einsum(
                    "kgts,skd->kgtd",
                    weights.astype(jnp.bfloat16),
                    value_rows,
                    preferred_element_type=jnp.float32,
                )
                accumulated = accumulated * decay[..., None] + update
                return (new_top, weight_sum, accumulated)

            def skipped(inner):
                return inner

            results.append(lax.cond(block_start <= last_pos, compute, skipped, state))
        return tuple(results)

    finals = lax.fori_loop(0, piece_rows // key_block, one_block, initial)
    parts = []
    for top_score, weight_sum, accumulated in finals:
        count = weight_sum.shape[2]
        rows = (accumulated / weight_sum[..., None]).astype(jnp.bfloat16)
        parts.append(rows.transpose(2, 0, 1, 3).reshape(count, heads_local * HD))
    attended = jnp.concatenate(parts, axis=0)
    returned = attended[half_rows:]
    for bit in range(lax.axis_size("sp").bit_length() - 1):
        returned = partner(returned, "sp", bit)
    attended = jnp.concatenate([attended[:half_rows], returned], axis=0)
    summed = sent_and_summed(
        jnp.dot(attended, w_out, preferred_element_type=jnp.float32).astype(jnp.bfloat16), "tp", 0
    )
    return summed.astype(jnp.bfloat16)


def solution(mesh):
    placed = (
        P(("sp", "tp"), None),
        P(None, "tp"),
        P(None, "tp"),
        P(None, "tp"),
        P("tp", None),
        P("tp", "sp"),
    )
    return jax.shard_map(
        per_device, mesh=mesh, in_specs=placed, out_specs=P(("sp", "tp"), None), check_vma=False
    )
```

profile of v0, /device:TPU:66, one launch (start us, length us, event | category | flops | bytes accessed | tf_op | source)
XLA Modules:
  0.0 399.5 jit_solution(4949304807565663179)
XLA Ops:
  7.7 19.5 %all_to_all.10 = bf16[4,64,2048]{2,1,0:T(8,128)(2,1)S(1)} all-to-all(bf16[4,64,2048]{2,1,0:T(8,128)(2,1)S(1)} %broadcast_in_dim.27), channel_id=1, replica_groups=mesh['sp'=128,'tp'=4] {'tp'}, dimensions={0} | all-to-all | bytes 2097152 | tf_op jit(solution)/shard_map/all_to_all | solution.py:13
  29.4 1.9 collective-permute-start
  31.3 1.2 collective-permute-done
  32.5 2.4 collective-permute-start.1
  35.0 3.7 collective-permute-done.1
  38.7 4.0 %collective-permute-start.2 = (bf16[128,256]{0,1:T(8,128)(2,1)S(1)}, bf16[128,256]{0,1:T(8,128)(2,1)S(1)}, u32[]{:S(2)}, u32[]{:S(2)}) collective-permute-start(bf16[128,256]{0,1:T(8,128)(2,1)S(1)} %collective-permute-done.1), channel_id=1, source_target_pairs={{0,16},{16,0},{4,20},{20,4},{8,24},{24,8},{12,28},{28,12},{32,48},... | collective-permute-start | bytes 196616 | tf_op jit(solution)/shard_map/ppermute | solution.py:34
  42.7 3.6 collective-permute-done.2
  46.3 3.8 collective-permute-start.3
  50.2 2.3 collective-permute-done.3
  52.5 1.9 collective-permute-start.4
  55.7 3.9 collective-permute-done.4
  59.6 9.4 %collective-permute-start.5 = (bf16[128,256]{0,1:T(8,128)(2,1)S(1)}, bf16[128,256]{0,1:T(8,128)(2,1)S(1)}, u32[]{:S(2)}, u32[]{:S(2)}) collective-permute-start(bf16[128,256]{0,1:T(8,128)(2,1)S(1)} %collective-permute-done.4), channel_id=1, source_target_pairs={{0,128},{128,0},{4,132},{132,4},{8,136},{136,8},{12,140},{140,12},... | collective-permute-start | bytes 196616 | tf_op jit(solution)/shard_map/ppermute | solution.py:34
  69.0 83.3 %all_gather.7 = f32[4,32768]{1,0:T(4,128)S(1)} all-gather(f32[4,256]{1,0:T(4,128)S(1)} %copy-done.4), channel_id=1, replica_groups=mesh['sp'=128,'tp'=4] {'sp'}, dimensions={1}, use_global_device_ids=true | all-gather | bytes 528384 | tf_op jit(solution)/shard_map/all_gather | solution.py:64
  152.3 7.3 %collective-permute-start.6 = (bf16[128,256]{0,1:T(8,128)(2,1)S(1)}, bf16[128,256]{0,1:T(8,128)(2,1)S(1)}, u32[]{:S(2)}, u32[]{:S(2)}) collective-permute-start(bf16[128,256]{0,1:T(8,128)(2,1)S(1)} %collective-permute-done.5), channel_id=1, source_target_pairs={{0,256},{256,0},{4,260},{260,4},{8,264},{264,8},{12,268},{268,12},... | collective-permute-start | bytes 196616 | tf_op jit(solution)/shard_map/ppermute | solution.py:34
  159.7 7.7 %collective-permute-done.6 = bf16[128,256]{0,1:T(8,128)(2,1)S(1)} collective-permute-done((bf16[128,256]{0,1:T(8,128)(2,1)S(1)}, bf16[128,256]{0,1:T(8,128)(2,1)S(1)}, u32[]{:S(2)}, u32[]{:S(2)}) %collective-permute-start.6) | collective-permute-done | bytes 65568 | tf_op jit(solution)/shard_map/ppermute | solution.py:34
  167.4 15.7 %all-gather.2.cloned.1.call-done = bf16[32768,128]{0,1:T(8,128)(2,1)} async-done(((bf16[256,128]{0,1:T(8,128)(2,1)}), bf16[32768,128]{0,1:T(8,128)(2,1)}) %all-gather.2.cloned.1.call-update) | async-done | bytes 8388624 | tf_op jit(solution)/shard_map/all_gather | solution.py:97
  183.1 134.2 %while.24 = (s32[]{:T(128)}, f32[1,4,128]{2,1,0:T(4,128)S(1)}, f32[1,4,128]{2,1,0:T(4,128)S(1)}, f32[1,4,128,64]{2,3,1,0:T(8,128)S(1)}, f32[1,4,128]{2,1,0:T(4,1...) while((s32[]{:T(128)}, f32[1,4,128]{2,1,0:T(4,128)S(1)}, ...), condition=%wide.region_11.12_spmd.clone, body=%wide.region_2.11_spmd.clone.sunk | while | flops 278270080 | bytes 14961743 | solution.py:142
  184.8 1.8 conditional.6
  187.2 1.8 conditional.7
  190.7 1.8 conditional.6
  193.2 1.8 conditional.7
  196.6 1.8 conditional.6
  199.1 1.8 conditional.7
  202.5 1.8 conditional.6
  205.0 1.8 conditional.7
  208.5 1.8 conditional.6
  210.9 1.8 conditional.7
  215.0 1.8 conditional.7
  219.2 1.8 conditional.7
  223.3 1.8 conditional.7
  227.4 1.8 conditional.7
  231.6 1.8 conditional.7
  235.7 1.8 conditional.7
  239.9 1.8 conditional.7
  244.0 1.8 conditional.7
  248.1 1.8 conditional.7
  252.3 1.8 conditional.7
  256.4 1.8 conditional.7
  260.5 1.8 conditional.7
  264.7 1.8 conditional.7
  268.8 1.8 conditional.7
  273.0 1.8 conditional.7
  277.1 1.8 conditional.7
  281.2 1.8 conditional.7
  285.4 1.8 conditional.7
  289.5 1.8 conditional.7
  293.7 1.8 conditional.7
  297.8 1.8 conditional.7
  301.9 1.8 conditional.7
  306.1 1.8 conditional.7
  317.3 2.2 collective-permute-start.7
  320.5 3.8 collective-permute-start.8
  324.3 2.5 collective-permute-done.8
  326.9 3.7 collective-permute-start.9
  330.5 4.0 collective-permute-done.9
  334.5 3.5 collective-permute-start.10
  338.0 2.7 collective-permute-done.10
  340.7 3.1 collective-permute-start.11
  343.8 4.0 collective-permute-done.11
  347.8 7.2 %collective-permute-start.12 = (bf16[128,256]{0,1:T(8,128)(2,1)S(1)}, bf16[128,256]{0,1:T(8,128)(2,1)S(1)}, u32[]{:S(2)}, u32[]{:S(2)}) collective-permute-start(bf16[128,256]{0,1:T(8,128)(2,1)S(1)} %collective-permute-done.11), channel_id=1, source_target_pairs={{0,128},{128,0},{4,132},{132,4},{8,136},{136,8},{12,140},{140,12},... | collective-permute-start | bytes 196616 | tf_op jit(solution)/shard_map/ppermute | solution.py:34
  354.9 3.0 collective-permute-done.12
  357.9 6.5 %collective-permute-start.13 = (bf16[128,256]{0,1:T(8,128)(2,1)S(1)}, bf16[128,256]{0,1:T(8,128)(2,1)S(1)}, u32[]{:S(2)}, u32[]{:S(2)}) collective-permute-start(bf16[128,256]{0,1:T(8,128)(2,1)S(1)} %collective-permute-done.12), channel_id=1, source_target_pairs={{0,256},{256,0},{4,260},{260,4},{8,264},{264,8},{12,268},{268,12},... | collective-permute-start | bytes 196616 | tf_op jit(solution)/shard_map/ppermute | solution.py:34
  364.5 9.1 %collective-permute-done.13 = bf16[128,256]{0,1:T(8,128)(2,1)S(1)} collective-permute-done((bf16[128,256]{0,1:T(8,128)(2,1)S(1)}, bf16[128,256]{0,1:T(8,128)(2,1)S(1)}, u32[]{:S(2)}, u32[]{:S(2)}) %collective-permute-start.13) | collective-permute-done | bytes 65568 | tf_op jit(solution)/shard_map/ppermute | solution.py:34
  374.1 17.7 %all_to_all.11 = bf16[4,64,2048]{2,1,0:T(8,128)(2,1)S(1)} all-to-all(bf16[4,64,2048]{2,1,0:T(8,128)(2,1)S(1)} %bitcast.112), channel_id=1, replica_groups=mesh['sp'=128,'tp'=4] {'tp'}, dimensions={0} | all-to-all | bytes 2097152 | tf_op jit(solution)/shard_map/all_to_all | solution.py:44
  (453 shorter events, 97.4 us)
Async XLA Ops:
  6.5 367.1 %copy-start = (bf16[256,2048]{1,0:T(8,128)(2,1)S(1)}, bf16[256,2048]{1,0:T(8,128)(2,1)}, u32[]{:S(2)}) copy-start(bf16[256,2048]{1,0:T(8,128)(2,1)} %param.16) | copy-start | bytes 3145732
  6.5 20.7 %copy-start.2 = (bf16[2048,64]{0,1:T(8,128)(2,1)S(1)}, bf16[2048,64]{0,1:T(8,128)(2,1)}, u32[]{:S(2)}) copy-start(bf16[2048,64]{0,1:T(8,128)(2,1)} %param.15) | copy-start | bytes 786436
  6.5 176.5 %all-gather.2.cloned.1.call-start = ((), (), s32[]{:S(2)}) async-start(), calls=%async_computation.2 | async-start | bytes 8454144 | tf_op jit(solution)/shard_map/all_gather | solution.py:97
  6.5 21.1 %copy-start.3 = (bf16[2048,64]{0,1:T(8,128)(2,1)S(1)}, bf16[2048,64]{0,1:T(8,128)(2,1)}, u32[]{:S(2)}) copy-start(bf16[2048,64]{0,1:T(8,128)(2,1)} %param.14) | copy-start | bytes 786436
  7.7 21.1 %copy-start.1 = (bf16[2048,256]{1,0:T(8,128)(2,1)S(1)}, bf16[2048,256]{1,0:T(8,128)(2,1)}, u32[]{:S(2)}) copy-start(bf16[2048,256]{1,0:T(8,128)(2,1)} %param.13) | copy-start | bytes 3145732
  27.7 15.0 %copy-start.4 = (f32[4,256]{1,0:T(4,128)S(1)}, f32[4,256]{1,0:T(4,128)}, u32[]{:S(2)}) copy-start(f32[4,256]{1,0:T(4,128)} %param.17) | copy-start | bytes 12292
  29.4 3.1 collective-permute-start
  32.5 6.1 %collective-permute-start.1 = (bf16[128,256]{0,1:T(8,128)(2,1)S(1)}, bf16[128,256]{0,1:T(8,128)(2,1)S(1)}, u32[]{:S(2)}, u32[]{:S(2)}) collective-permute-start(bf16[128,256]{0,1:T(8,128)(2,1)S(1)} %collective-permute-done), channel_id=1, source_target_pairs={{0,8},{8,0},{4,12},{12,4},{16,24},{24,16},{20,28},{28,20},{32,40},... | collective-permute-start | bytes 196616 | tf_op jit(solution)/shard_map/ppermute | solution.py:34
  38.7 7.7 %collective-permute-start.2 = (bf16[128,256]{0,1:T(8,128)(2,1)S(1)}, bf16[128,256]{0,1:T(8,128)(2,1)S(1)}, u32[]{:S(2)}, u32[]{:S(2)}) collective-permute-start(bf16[128,256]{0,1:T(8,128)(2,1)S(1)} %collective-permute-done.1), channel_id=1, source_target_pairs={{0,16},{16,0},{4,20},{20,4},{8,24},{24,8},{12,28},{28,12},{32,48},... | collective-permute-start | bytes 196616 | tf_op jit(solution)/shard_map/ppermute | solution.py:34
  46.3 6.1 %collective-permute-start.3 = (bf16[128,256]{0,1:T(8,128)(2,1)S(1)}, bf16[128,256]{0,1:T(8,128)(2,1)S(1)}, u32[]{:S(2)}, u32[]{:S(2)}) collective-permute-start(bf16[128,256]{0,1:T(8,128)(2,1)S(1)} %collective-permute-done.2), channel_id=1, source_target_pairs={{0,32},{32,0},{4,36},{36,4},{8,40},{40,8},{12,44},{44,12},{16,48},... | collective-permute-start | bytes 196616 | tf_op jit(solution)/shard_map/ppermute | solution.py:34
  52.5 7.1 %collective-permute-start.4 = (bf16[128,256]{0,1:T(8,128)(2,1)S(1)}, bf16[128,256]{0,1:T(8,128)(2,1)S(1)}, u32[]{:S(2)}, u32[]{:S(2)}) collective-permute-start(bf16[128,256]{0,1:T(8,128)(2,1)S(1)} %collective-permute-done.3), channel_id=1, source_target_pairs={{0,64},{64,0},{4,68},{68,4},{8,72},{72,8},{12,76},{76,12},{16,80},... | collective-permute-start | bytes 196616 | tf_op jit(solution)/shard_map/ppermute | solution.py:34
  59.6 92.7 %collective-permute-start.5 = (bf16[128,256]{0,1:T(8,128)(2,1)S(1)}, bf16[128,256]{0,1:T(8,128)(2,1)S(1)}, u32[]{:S(2)}, u32[]{:S(2)}) collective-permute-start(bf16[128,256]{0,1:T(8,128)(2,1)S(1)} %collective-permute-done.4), channel_id=1, source_target_pairs={{0,128},{128,0},{4,132},{132,4},{8,136},{136,8},{12,140},{140,12},... | collective-permute-start | bytes 196616 | tf_op jit(solution)/shard_map/ppermute | solution.py:34
  152.3 15.1 %collective-permute-start.6 = (bf16[128,256]{0,1:T(8,128)(2,1)S(1)}, bf16[128,256]{0,1:T(8,128)(2,1)S(1)}, u32[]{:S(2)}, u32[]{:S(2)}) collective-permute-start(bf16[128,256]{0,1:T(8,128)(2,1)S(1)} %collective-permute-done.5), channel_id=1, source_target_pairs={{0,256},{256,0},{4,260},{260,4},{8,264},{264,8},{12,268},{268,12},... | collective-permute-start | bytes 196616 | tf_op jit(solution)/shard_map/ppermute | solution.py:34
  317.3 3.1 collective-permute-start.7
  320.5 6.4 %collective-permute-start.8 = (bf16[128,256]{0,1:T(8,128)(2,1)S(1)}, bf16[128,256]{0,1:T(8,128)(2,1)S(1)}, u32[]{:S(2)}, u32[]{:S(2)}) collective-permute-start(bf16[128,256]{0,1:T(8,128)(2,1)S(1)} %collective-permute-done.7), channel_id=1, source_target_pairs={{0,8},{8,0},{4,12},{12,4},{16,24},{24,16},{20,28},{28,20},{32,40},... | collective-permute-start | bytes 196616 | tf_op jit(solution)/shard_map/ppermute | solution.py:34
  326.9 7.7 %collective-permute-start.9 = (bf16[128,256]{0,1:T(8,128)(2,1)S(1)}, bf16[128,256]{0,1:T(8,128)(2,1)S(1)}, u32[]{:S(2)}, u32[]{:S(2)}) collective-permute-start(bf16[128,256]{0,1:T(8,128)(2,1)S(1)} %collective-permute-done.8), channel_id=1, source_target_pairs={{0,16},{16,0},{4,20},{20,4},{8,24},{24,8},{12,28},{28,12},{32,48},... | collective-permute-start | bytes 196616 | tf_op jit(solution)/shard_map/ppermute | solution.py:34
  334.5 6.1 %collective-permute-start.10 = (bf16[128,256]{0,1:T(8,128)(2,1)S(1)}, bf16[128,256]{0,1:T(8,128)(2,1)S(1)}, u32[]{:S(2)}, u32[]{:S(2)}) collective-permute-start(bf16[128,256]{0,1:T(8,128)(2,1)S(1)} %collective-permute-done.9), channel_id=1, source_target_pairs={{0,32},{32,0},{4,36},{36,4},{8,40},{40,8},{12,44},{44,12},{16,48},... | collective-permute-start | bytes 196616 | tf_op jit(solution)/shard_map/ppermute | solution.py:34
  340.7 7.1 %collective-permute-start.11 = (bf16[128,256]{0,1:T(8,128)(2,1)S(1)}, bf16[128,256]{0,1:T(8,128)(2,1)S(1)}, u32[]{:S(2)}, u32[]{:S(2)}) collective-permute-start(bf16[128,256]{0,1:T(8,128)(2,1)S(1)} %collective-permute-done.10), channel_id=1, source_target_pairs={{0,64},{64,0},{4,68},{68,4},{8,72},{72,8},{12,76},{76,12},{16,80},... | collective-permute-start | bytes 196616 | tf_op jit(solution)/shard_map/ppermute | solution.py:34
  347.8 10.2 %collective-permute-start.12 = (bf16[128,256]{0,1:T(8,128)(2,1)S(1)}, bf16[128,256]{0,1:T(8,128)(2,1)S(1)}, u32[]{:S(2)}, u32[]{:S(2)}) collective-permute-start(bf16[128,256]{0,1:T(8,128)(2,1)S(1)} %collective-permute-done.11), channel_id=1, source_target_pairs={{0,128},{128,0},{4,132},{132,4},{8,136},{136,8},{12,140},{140,12},... | collective-permute-start | bytes 196616 | tf_op jit(solution)/shard_map/ppermute | solution.py:34
  357.9 15.7 %collective-permute-start.13 = (bf16[128,256]{0,1:T(8,128)(2,1)S(1)}, bf16[128,256]{0,1:T(8,128)(2,1)S(1)}, u32[]{:S(2)}, u32[]{:S(2)}) collective-permute-start(bf16[128,256]{0,1:T(8,128)(2,1)S(1)} %collective-permute-done.12), channel_id=1, source_target_pairs={{0,256},{256,0},{4,260},{260,4},{8,264},{264,8},{12,268},{268,12},... | collective-permute-start | bytes 196616 | tf_op jit(solution)/shard_map/ppermute | solution.py:34
Sparse Core Ops, SparseCore 0:
  28.9 154.0 all-gather.1
where the time goes:
time: 401 us; the launch traced here: 400 us
  blocking collectives  121 us (30%)
  waiting for transfers between devices  64.4 us (16%)
  starting transfers between devices  60.8 us (15%)
  loops' own time  44.4 us (11%)
  matrix products  41.9 us (10%)
  local copies, waits for them, and re-layouts  33.5 us (8%)
  other arithmetic  20.3 us (5%)
  between operations  13.7 us (3%)
    all_gather x1, blocking collectives, per_device(): gate_all = lax.all_gather(cum_gate, 'sp', axis=1, tiled=True)  83.3 us
    ppermute x14, starting transfers between devices, partner(): return lax.ppermute(block, axis, route)  60.8 us
    ppermute x14, waiting for transfers between devices, partner(): return lax.ppermute(block, axis, route)  48.7 us
    another operation x1, loops' own time, per_device(): finals = lax.fori_loop(0, piece_rows // key_block, one_block, initial)  41.9 us
    reshape x32, local copies, waits for them, and re-layouts, one_block(): value_rows = slab[:, kv_local * HD:].reshape(key_block, kv_local, HD)  31.8 us
    dot_general x33, matrix products, compute(): jnp.einsum('tkgd,skd->kgts', queries, key_rows, preferred_element_type=jn...  24.4 us
    all_to_all x1, blocking collectives, sent_to_all(): return lax.all_to_all(copies, axis, split_axis=0, concat_axis=0, tiled=True)  19.5 us
    all_to_all x1, blocking collectives, sent_and_summed(): parts = lax.all_to_all(cut_along(x, dim, peers), axis, 0, 0, tiled=True)  17.7 us
  transfers between devices with their start and end apart: 15, of which 14 were waited for; matrix products, arithmetic and copies ran while one was open for 0% of the time, Pallas kernels for 0%

commit v1 on v0

v1 whole, which is shorter than its diff:
```python
import functools

import jax
import jax.numpy as jnp
from jax import lax
from jax.experimental import pallas as pl
from jax.experimental.pallas import tpu as pltpu
from jax.sharding import Mesh, PartitionSpec as P

HD = 64
ROWS = 256
HALF = 128
GROUP = 4
KROWS = 80
VROWS = 72
NEG_START = -1e30
NEG_MASKED = -2e30
BF = jnp.bfloat16
F32 = jnp.float32
SWAP = ((0, 1), (1, 0))
VMEM = pl.BlockSpec(memory_space=pltpu.VMEM)
SMEM = pl.BlockSpec(memory_space=pltpu.SMEM)


def three_parts(x):
    high = x.astype(BF)
    rest = x - high.astype(F32)
    middle = rest.astype(BF)
    low = (rest - middle.astype(F32)).astype(BF)
    return high, middle, low


def project_kernel(x_ref, wq_ref, wk_ref, wv_ref, gate_ref, q_ref, kv_ref):
    x = x_ref[...]
    query = jnp.dot(x, wq_ref[...], preferred_element_type=F32)
    for part in range(2):
        rows = [query[y * 64 + part * 32 : y * 64 + part * 32 + 32] for y in range(4)]
        turned = jnp.concatenate(rows, axis=0).T.astype(BF)
        q_ref[part] = (turned.astype(F32) * 0.125).astype(BF)
    kv_ref[0:64] = jnp.dot(x, wk_ref[...], preferred_element_type=F32).T.astype(BF)
    kv_ref[KROWS : KROWS + 64] = jnp.dot(x, wv_ref[...], preferred_element_type=F32).T.astype(BF)
    high, middle, low = three_parts(-gate_ref[...])
    kv_ref[64:80] = jnp.concatenate([high, middle, low, jnp.zeros((4, ROWS), BF)], axis=0)


def project(x, w_query, w_key, w_value, gate):
    return pl.pallas_call(
        project_kernel,
        in_specs=[VMEM] * 5,
        out_specs=[VMEM] * 2,
        out_shape=[
            jax.ShapeDtypeStruct((2, GROUP * HD, HALF), BF),
            jax.ShapeDtypeStruct((KROWS + 64, ROWS), BF),
        ],
        cost_estimate=pl.CostEstimate(flops=2 * 256 * 2048 * 384, bytes_accessed=3 << 20, transcendentals=0),
        name="project",
    )(x, w_query, w_key, w_value, gate)


def attend_kernel(first, last, sc_ref, q_ref, kv_ref, *refs):
    if first:
        refs = list(refs)
    else:
        acc_in, top_in, *refs = refs
    if last:
        out_ref, acc, top, qa, ks, vs = refs
    else:
        acc, top, qa, ks, vs = refs
    if first:
        acc[...] = jnp.zeros_like(acc)
        top[...] = jnp.full(top.shape, NEG_START, F32)
    else:
        acc[...] = acc_in[...]
        top[...] = top_in[...]
    row = lax.broadcasted_iota(jnp.int32, (16, 512), 0)
    head = lax.broadcasted_iota(jnp.int32, (16, 512), 1) // HALF
    chooser = jnp.where((row < 12) & (row % 4 == head), 1.0, 0.0).astype(BF)
    for part in range(2):
        for xq in range(4):
            for h in range(GROUP):
                qa[part, xq, 0:64, h * HALF : (h + 1) * HALF] = q_ref[xq, part, h * HD : (h + 1) * HD, :]
            qa[part, xq, 64:80, :] = chooser
    for b in range(8):
        ks[b * ROWS : (b + 1) * ROWS, 0:KROWS] = kv_ref[b, 0:KROWS, :].astype(F32).T.astype(BF)
        vs[b, 0:64] = kv_ref[b, KROWS : KROWS + 64, :]
        vs[b, 64:72] = jnp.ones((8, ROWS), BF)

    def step(part, block, count, start):
        keys = ks[pl.ds(pl.multiple_of(block * ROWS, ROWS), count * ROWS), 0:KROWS]
        for xq in range(4):
            for side in range(2):
                cols = slice(side * 256, side * 256 + 256)
                scores = jnp.dot(keys, qa[part, xq, :, cols], preferred_element_type=F32)
                if start is not None:
                    key_pos = start + lax.broadcasted_iota(jnp.int32, scores.shape, 0)
                    lane = lax.broadcasted_iota(jnp.int32, (1, 256), 1) % HALF
                    query_pos = xq * 512 + sc_ref[5] + part * 32 + (lane // 32) * 64 + lane % 32
                    scores = jnp.where(key_pos <= query_pos, scores, NEG_MASKED)
                old = top[part, xq, :, cols]
                new = jnp.maximum(old, jnp.max(scores, axis=0, keepdims=True))
                weights = jnp.exp(scores - new).astype(BF)
                decay = jnp.exp(old - new)
                update = jnp.dot(vs[block], weights[0:ROWS], preferred_element_type=F32)
                for j in range(1, count):
                    update += jnp.dot(vs[block + j], weights[j * ROWS : (j + 1) * ROWS], preferred_element_type=F32)
                acc[part, xq, :, cols] = acc[part, xq, :, cols] * decay + update
                top[part, xq, :, cols] = new

    def one_part(part, carry):
        full = sc_ref[part]
        pairs = full // 2

        def pair(i, c):
            step(part, i * 2, 2, None)
            return c

        def single(i, c):
            step(part, i, 1, jnp.where(i < full, -1000000, sc_ref[4]))
            return c

        lax.fori_loop(0, pairs, pair, 0)
        lax.fori_loop(pairs * 2, full + sc_ref[2 + part], single, 0)
        return carry

    lax.fori_loop(0, 2, one_part, 0)
    if last:
        for part in range(2):
            for xq in range(4):
                total = acc[part, xq, 64:65, :]
                some = total > 0.0
                safe = jnp.where(some, total, 1.0)
                out_ref[xq, part, 0:64] = (acc[part, xq, 0:64, :] / safe).astype(BF)
                level = jnp.where(some, top[part, xq] + jnp.log(safe), NEG_START)
                high, middle, low = three_parts(level)
                out_ref[xq, part, 64:72] = jnp.concatenate([high, middle, low, jnp.zeros((5, 512), BF)], axis=0)


def attend(scalars, queries, kv, state, last):
    first = state is None
    args = [scalars, queries, kv] + ([] if first else list(state))
    acc_shape = (2, 4, VROWS, 512)
    top_shape = (2, 4, 1, 512)
    scratch = [
        pltpu.VMEM((2, 4, KROWS, 512), BF),
        pltpu.VMEM((8 * ROWS, 128), BF),
        pltpu.VMEM((8, VROWS, ROWS), BF),
    ]
    if last:
        out_shape = [jax.ShapeDtypeStruct((4, 2, VROWS, 512), BF)]
        scratch = [pltpu.VMEM(acc_shape, F32), pltpu.VMEM(top_shape, F32)] + scratch
    else:
        out_shape = [jax.ShapeDtypeStruct(acc_shape, F32), jax.ShapeDtypeStruct(top_shape, F32)]
    return pl.pallas_call(
        functools.partial(attend_kernel, first, last),
        in_specs=[SMEM] + [VMEM] * (len(args) - 1),
        out_specs=[VMEM] * len(out_shape),
        out_shape=out_shape,
        scratch_shapes=scratch,
        cost_estimate=pl.CostEstimate(flops=5_000_000_000, bytes_accessed=4 << 20, transcendentals=4 << 20),
        compiler_params=pltpu.CompilerParams(vmem_limit_bytes=40 << 20),
        name="attend",
    )(*args)


def combine_kernel(x_ref, o_ref):
    for part in range(2):
        levels = []
        for s in range(4):
            high, middle, low = (x_ref[s, part, 64 + j : 65 + j, :].astype(F32) for j in range(3))
            levels.append(high + middle + low)
        top = jnp.maximum(jnp.maximum(levels[0], levels[1]), jnp.maximum(levels[2], levels[3]))
        shares = [jnp.exp(level - top) for level in levels]
        total = shares[0] + shares[1] + shares[2] + shares[3]
        mixed = x_ref[0, part, 0:64, :].astype(F32) * shares[0]
        for s in range(1, 4):
            mixed += x_ref[s, part, 0:64, :].astype(F32) * shares[s]
        mixed = (mixed / total).astype(BF)
        for h in range(GROUP):
            o_ref[part, h * HD : (h + 1) * HD, :] = mixed[:, h * HALF : (h + 1) * HALF]


def combine(x):
    return pl.pallas_call(
        combine_kernel,
        in_specs=[VMEM],
        out_specs=VMEM,
        out_shape=jax.ShapeDtypeStruct((2, GROUP * HD, HALF), BF),
        cost_estimate=pl.CostEstimate(flops=1_000_000, bytes_accessed=1 << 20, transcendentals=0),
        name="combine",
    )(x)


def sent_to_all(x, axis):
    copies = jnp.broadcast_to(x, (lax.axis_size(axis), *x.shape))
    return lax.all_to_all(copies, axis, split_axis=0, concat_axis=0, tiled=True)


def per_device(tokens, w_query, w_key, w_value, w_out, cum_gate):
    zh, zl, x, c = (lax.axis_index(a) for a in ("zh", "zl", "x", "c"))
    plane = zh * 2 + zl
    mirror = [(i, 15 - i) for i in range(16)]
    rows = sent_to_all(tokens, "y").reshape(ROWS, -1)
    queries, kv = project(rows, w_query, w_key, w_value, cum_gate)
    moved = lax.ppermute(queries[1], ("zh", "zl"), mirror)
    same_own = lax.all_gather(kv, "zh", axis=0)
    other_own = lax.ppermute(same_own, "zl", SWAP)
    same_swapped = lax.ppermute(same_own, "c", SWAP)
    other_swapped = lax.ppermute(other_own, "c", SWAP)
    gathered = sent_to_all(jnp.stack([queries[0], moved]), "x").reshape(4, 2, GROUP * HD, HALF)
    state = None
    blocks = [(same_own, zl, c), (same_swapped, zl, 1 - c), (other_own, 1 - zl, c), (other_swapped, 1 - zl, 1 - c)]
    for number, (block, parity, side) in enumerate(blocks):
        scalars = jnp.stack(
            [
                (plane - parity + 1) // 2,
                (15 - plane - parity + 1) // 2,
                1 - (plane - parity) % 2,
                1 - (15 - plane - parity) % 2,
                x * 512 + side * ROWS,
                c * ROWS,
            ]
        ).astype(jnp.int32)
        state = attend(scalars, gathered, block, state, number == 3)
    shared = lax.all_to_all(state[0], "x", 0, 0, tiled=True)
    mixed = combine(shared)
    back = lax.ppermute(mixed[1], ("zh", "zl"), mirror)
    outs = []
    for half in (mixed[0], back):
        share = lax.dot_general(half, w_out, (((0,), (0,)), ((), ())), preferred_element_type=F32).astype(BF)
        pieces = lax.all_to_all(share.reshape(4, 32, -1), "y", 0, 0, tiled=True)
        outs.append(jnp.sum(pieces.astype(F32), axis=0).astype(BF))
    return jnp.concatenate(outs, axis=0)


def solution(mesh):
    fine = Mesh(mesh.devices.reshape(8, 2, 4, 2, 4), ("zh", "zl", "x", "c", "y"))
    sp = ("zh", "zl", "x", "c")
    placed = (
        P((*sp, "y"), None),
        P(None, "y"),
        P(None, "y"),
        P(None, "y"),
        P("y", None),
        P("y", sp),
    )
    return jax.shard_map(per_device, mesh=fine, in_specs=placed, out_specs=P((*sp, "y"), None), check_vma=False)
```

time: 401 us -> 205 us (0.51)
  the two profiles are of different devices: /device:TPU:66 before, /device:TPU:64 now
where the time goes in v1:
time: 205 us; the launch traced here: 204 us
  Pallas kernels  71.7 us (35%)
  blocking collectives  49.2 us (24%)
  starting transfers between devices  42.3 us (21%)
  waiting for transfers between devices  29.2 us (14%)
  local copies, waits for them, and re-layouts  7.33 us (4%)
  matrix products  3.2 us (2%)
    pallas_call x4, Pallas kernels, attend(): pl.pallas_call(functools.partial(attend_kernel, first, last), in_specs=[S...  66.3 us
    all_gather x1, blocking collectives, per_device(): same_own = lax.all_gather(kv, 'zh', axis=0)  33.8 us
    all_to_all x1, blocking collectives, per_device(): shared = lax.all_to_all(state[0], 'x', 0, 0, tiled=True)  15.4 us
    all_to_all x2, waiting for transfers between devices, sent_to_all(): return lax.all_to_all(copies, axis, split_axis=0, concat_axis=0, tiled=True)  13 us
    ppermute x1, starting transfers between devices, per_device(): moved = lax.ppermute(queries[1], ('zh', 'zl'), mirror)  11.4 us
    all_to_all x2, starting transfers between devices, sent_to_all(): return lax.all_to_all(copies, axis, split_axis=0, concat_axis=0, tiled=True)  8.89 us
    all_to_all x2, starting transfers between devices, per_device(): pieces = lax.all_to_all(share.reshape(4, 32, -1), 'y', 0, 0, tiled=True)  8.21 us
    all_to_all x2, waiting for transfers between devices, per_device(): pieces = lax.all_to_all(share.reshape(4, 32, -1), 'y', 0, 0, tiled=True)  8 us
  transfers between devices with their start and end apart: 9, of which 4 were waited for; matrix products, arithmetic and copies ran while one was open for 2% of the time, Pallas kernels for 25%

profile of v1, /device:TPU:64, one launch (start us, length us, event | category | flops | bytes accessed | tf_op | source)
XLA Modules:
  0.0 204.1 jit_solution(874413880484889593)
XLA Ops:
  0.0 0.0 copy-start
  0.0 2.1 %broadcast_in_dim.6 = bf16[4,64,2048]{2,1,0:T(8,128)(2,1)} broadcast(bf16[64,2048]{1,0:T(8,128)(2,1)} %param.6), dimensions={1,2} | broadcast | bytes 1310720 | tf_op jit(solution)/shard_map/broadcast_in_dim | solution.py:194
  2.1 0.0 copy-start.3
  2.1 0.0 copy-start.4
  2.1 4.6 %all-to-all-start = ((bf16[4,64,2048]{2,1,0:T(8,128)(2,1)}), bf16[4,64,2048]{2,1,0:T(8,128)(2,1)S(1)}, u32[]{:S(2)}, u32[]{:S(2)}) async-start(bf16[4,64,2048]{2,1,0:T(8,128)(2,1)} %broadcast_in_dim.6), calls=%async_computation | async-start | bytes 2097152 | tf_op jit(solution)/shard_map/all_to_all | solution.py:195
  6.7 0.0 copy-done.3
  6.7 1.0 copy.7.wk_ref
  7.8 0.0 copy-done.4
  7.8 1.0 copy.8.wv_ref
  8.8 13.0 %all-to-all-done = bf16[4,64,2048]{2,1,0:T(8,128)(2,1)S(1)} async-done(((bf16[4,64,2048]{2,1,0:T(8,128)(2,1)}), bf16[4,64,2048]{2,1,0:T(8,128)(2,1)S(1)}, u32[]{:S(2)}, u32[]{:S(2)}) %all-to-all-start) | async-done | bytes 1048608 | tf_op jit(solution)/shard_map/all_to_all | solution.py:195
  21.8 0.0 copy-start.1
  21.8 1.0 copy-done.1
  22.8 3.5 %project.1 = (bf16[2,256,128]{2,1,0:T(8,128)(2,1)}, bf16[144,256]{1,0:T(8,128)(2,1)}) custom-call(bf16[256,2048]{1,0:T(8,128)(2,1)} %bitcast.29, bf16[2048,256]{1,0:T(8,128)(2,1)} %wq_ref.1, bf16[2048,64]{1,0:T(8,128)(2,1)} %copy.7.wk_ref, bf16[2048,64]{1,0:T(8,128)(2,1)} %copy.8.wv_ref, f32[4,256]{1,0:T(4,128)} %gate_ref.1), custom_call_target="tpu_custom_call" | custom-call | flops 402653184 | bytes 3145728 | tf_op jit(solution)/shard_map/project/pallas_call | solution.py:47
  26.3 0.0 copy-start.5
  26.3 0.9 fusion
  27.2 11.4 %collective-permute-start = (bf16[256,128]{1,0:T(8,128)(2,1)S(1)}, bf16[256,128]{1,0:T(8,128)(2,1)S(1)}, u32[]{:S(2)}, u32[]{:S(2)}) collective-permute-start(bf16[256,128]{1,0:T(8,128)(2,1)S(1)} %get-tuple-element.22), channel_id=1, source_target_pairs={{0,480},{32,448},{64,416},{96,384},{128,352},{160,320},{192,288},{... | collective-permute-start | bytes 196616 | tf_op jit(solution)/shard_map/ppermute | solution.py:204
  38.6 3.0 %collective-permute-done = bf16[256,128]{1,0:T(8,128)(2,1)S(1)} collective-permute-done((bf16[256,128]{1,0:T(8,128)(2,1)S(1)}, bf16[256,128]{1,0:T(8,128)(2,1)S(1)}, u32[]{:S(2)}, u32[]{:S(2)}) %collective-permute-start) | collective-permute-done | bytes 65568 | tf_op jit(solution)/shard_map/ppermute | solution.py:204
  41.6 0.9 broadcast_in_dim.7
  42.5 4.3 %all-to-all-start.1 = ((bf16[4,2,256,128]{3,2,1,0:T(8,128)(2,1)}), bf16[4,2,256,128]{3,2,1,0:T(8,128)(2,1)S(1)}, u32[]{:S(2)}, u32[]{:S(2)}) async-start(bf16[4,2,256,128]{3,2,1,0:T(8,128)(2,1)} %broadcast_in_dim.7), calls=%async_computation.1 | async-start | bytes 1048576 | tf_op jit(solution)/shard_map/all_to_all | solution.py:195
  46.8 0.0 copy-done.5
  46.8 33.8 %all-gather = bf16[1152,256]{1,0:T(8,128)(2,1)S(1)} all-gather(bf16[144,256]{1,0:T(8,128)(2,1)S(1)} %copy-done.5), channel_id=2, replica_groups=mesh['zh'=8,'zl'=2,'x'=4,'c'=2,'y'=4] {'zh'}, dimensions={0}, use_global_device_ids=true | all-gather | bytes 663552 | tf_op jit(solution)/shard_map/all_gather | solution.py:205
  80.6 3.5 %collective-permute-start.1 = (bf16[8,144,256]{2,1,0:T(8,128)(2,1)S(1)}, bf16[8,144,256]{2,1,0:T(8,128)(2,1)S(1)}, u32[]{:S(2)}, u32[]{:S(2)}) collective-permute-start(bf16[8,144,256]{2,1,0:T(8,128)(2,1)S(1)} %bitcast.26), channel_id=1, source_target_pairs={{0,32},{32,0},{1,33},{33,1},{2,34},{34,2},{3,35},{35,3},{4,36},{36... | collective-permute-start | bytes 1769480 | tf_op jit(solution)/shard_map/ppermute | solution.py:206
  84.2 1.9 collective-permute-start.3
  86.2 0.1 stack.80.sc_ref
  86.3 0.1 stack.79.sc_ref
  86.3 0.1 stack.74.sc_ref
  86.4 0.1 stack.70.sc_ref
  86.5 0.0 all-to-all-done.1.q_ref
  86.5 17.7 %attend.4 = (f32[2,4,72,512]{3,2,1,0:T(8,128)S(1)}, f32[2,4,1,512]{3,2,1,0:T(1,128)S(1)}) custom-call(s32[6]{0:T(128)S(1)} %stack.80.sc_ref, bf16[4,2,256,128]{3,2,1,0:T(8,128)(2,1)S(1)} %all-to-all-done.1.q_ref, bf16[8,144,256]{2,1,0:T(8,128)(2,1)S(1)} %bitcast.28), custom_call_target="tpu_custom_call" | custom-call | flops 5000000000 | bytes 4194304 | tf_op jit(solution)/shard_map/attend/pallas_call | solution.py:153
  104.2 0.0 collective-permute-done.1.kv_ref
  104.2 2.6 %collective-permute-start.2 = (bf16[8,144,256]{2,1,0:T(8,128)(2,1)S(1)}, bf16[8,144,256]{2,1,0:T(8,128)(2,1)S(1)}, u32[]{:S(2)}, u32[]{:S(2)}) collective-permute-start(bf16[8,144,256]{2,1,0:T(8,128)(2,1)S(1)} %collective-permute-done.1.kv_ref), channel_id=1, source_target_pairs={{0,4},{4,0},{1,5},{5,1},{2,6},{6,2},{3,7},{7,3},{8,12},{12,8},{9,1... | collective-permute-start | bytes 1769480 | tf_op jit(solution)/shard_map/ppermute | solution.py:208
  106.8 0.0 collective-permute-done.3.kv_ref
  106.8 17.7 %attend.5 = (f32[2,4,72,512]{3,2,1,0:T(8,128)S(1)}, f32[2,4,1,512]{3,2,1,0:T(1,128)S(1)}) custom-call(s32[6]{0:T(128)S(1)} %stack.79.sc_ref, bf16[4,2,256,128]{3,2,1,0:T(8,128)(2,1)S(1)} %all-to-all-done.1.q_ref, bf16[8,144,256]{2,1,0:T(8,128)(2,1)S(1)} %collective-permute-done.3.kv_ref, f32[2,4,72,512]{3,2,1,0:T(8,128)S(1)} %get-tuple-element.15.refs_0_, ...), custom_call_target="tpu_custom_call" | custom-call | flops 5000000000 | bytes 4194304 | tf_op jit(solution)/shard_map/attend/pallas_call | solution.py:153
  124.5 15.4 %attend.6 = (f32[2,4,72,512]{3,2,1,0:T(8,128)S(1)}, f32[2,4,1,512]{3,2,1,0:T(1,128)S(1)}) custom-call(s32[6]{0:T(128)S(1)} %stack.74.sc_ref, bf16[4,2,256,128]{3,2,1,0:T(8,128)(2,1)S(1)} %all-to-all-done.1.q_ref, bf16[8,144,256]{2,1,0:T(8,128)(2,1)S(1)} %collective-permute-done.1.kv_ref, f32[2,4,72,512]{3,2,1,0:T(8,128)S(1)} %get-tuple-element.17.refs_0_, ...), custom_call_target="tpu_custom_call" | custom-call | flops 5000000000 | bytes 4194304 | tf_op jit(solution)/shard_map/attend/pallas_call | solution.py:153
  139.9 0.0 collective-permute-done.2.kv_ref
  139.9 15.6 %attend.7 = bf16[4,2,72,512]{3,2,1,0:T(8,128)(2,1)S(1)} custom-call(s32[6]{0:T(128)S(1)} %stack.70.sc_ref, bf16[4,2,256,128]{3,2,1,0:T(8,128)(2,1)S(1)} %all-to-all-done.1.q_ref, bf16[8,144,256]{2,1,0:T(8,128)(2,1)S(1)} %collective-permute-done.2.kv_ref, f32[2,4,72,512]{3,2,1,0:T(8,128)S(1)} %get-tuple-element.19.refs_0_, ...), custom_call_target="tpu_custom_call" | custom-call | flops 5000000000 | bytes 4194304 | tf_op jit(solution)/shard_map/attend/pallas_call | solution.py:153
  155.5 15.4 %all_to_all.25.x_ref = bf16[4,2,72,512]{3,2,1,0:T(8,128)(2,1)} all-to-all(bf16[4,2,72,512]{3,2,1,0:T(8,128)(2,1)S(1)} %attend.7), channel_id=1, replica_groups=mesh['zh'=8,'zl'=2,'x'=4,'c'=2,'y'=4] {'x'}, dimensions={0} | all-to-all | bytes 1179648 | tf_op jit(solution)/shard_map/all_to_all | solution.py:224
  170.9 1.9 combine.1
  172.8 0.0 copy-done
  172.8 0.0 copy-start.2
  172.8 2.0 %convolution_convert_fusion.1 = bf16[128,2048]{1,0:T(8,128)(2,1)} fusion(bf16[256,2048]{1,0:T(8,128)(2,1)S(1)} %copy-done, bf16[2,256,128]{2,1,0:T(8,128)(2,1)} %combine.1), kind=kOutput, calls=%fused_computation.1 | convolution fusion | flops 134479872 | bytes 1638400 | tf_op jit(solution)/shard_map/dot_general | solution.py:229
  174.8 3.5 %all-to-all-start.3 = ((bf16[4,32,2048]{2,1,0:T(8,128)(2,1)}), bf16[4,32,2048]{2,1,0:T(8,128)(2,1)S(1)}, u32[]{:S(2)}, u32[]{:S(2)}) async-start(bf16[4,32,2048]{2,1,0:T(8,128)(2,1)} %bitcast.16), calls=%async_computation.3 | async-start | bytes 1048576 | tf_op jit(solution)/shard_map/all_to_all | solution.py:230
  178.3 0.0 copy-done.2
  178.3 5.8 %collective-permute-start.4 = (bf16[256,128]{1,0:T(8,128)(2,1)S(1)}, bf16[256,128]{1,0:T(8,128)(2,1)S(1)}, u32[]{:S(2)}, u32[]{:S(2)}) collective-permute-start(bf16[256,128]{1,0:T(8,128)(2,1)S(1)} %slice_bitcast_fusion), channel_id=1, source_target_pairs={{0,480},{32,448},{64,416},{96,384},{128,352},{160,320},{192,288},{... | collective-permute-start | bytes 196616 | tf_op jit(solution)/shard_map/ppermute | solution.py:226
  184.2 5.2 %collective-permute-done.4 = bf16[256,128]{1,0:T(8,128)(2,1)S(1)} collective-permute-done((bf16[256,128]{1,0:T(8,128)(2,1)S(1)}, bf16[256,128]{1,0:T(8,128)(2,1)S(1)}, u32[]{:S(2)}, u32[]{:S(2)}) %collective-permute-start.4) | collective-permute-done | bytes 65568 | tf_op jit(solution)/shard_map/ppermute | solution.py:226
  189.3 1.1 convolution_convert_fusion
  190.5 0.0 all-to-all-done.3
  190.5 4.7 %all-to-all-start.4 = ((bf16[4,32,2048]{2,1,0:T(8,128)(2,1)}), bf16[4,32,2048]{2,1,0:T(8,128)(2,1)S(1)}, u32[]{:S(2)}, u32[]{:S(2)}) async-start(bf16[4,32,2048]{2,1,0:T(8,128)(2,1)} %bitcast.18), calls=%async_computation.4 | async-start | bytes 1048576 | tf_op jit(solution)/shard_map/all_to_all | solution.py:230
  195.2 0.1 reduce_sum.24
  195.3 8.0 %all-to-all-done.4 = bf16[4,32,2048]{2,1,0:T(8,128)(2,1)S(1)} async-done(((bf16[4,32,2048]{2,1,0:T(8,128)(2,1)}), bf16[4,32,2048]{2,1,0:T(8,128)(2,1)S(1)}, u32[]{:S(2)}, u32[]{:S(2)}) %all-to-all-start.4) | async-done | bytes 524320 | tf_op jit(solution)/shard_map/all_to_all | solution.py:230
  203.3 0.1 reduce_sum.25
  203.4 0.7 pad_maximum_fusion
  (2 shorter events, 0.0 us)
Async XLA Ops:
  0.0 172.8 %copy-start = (bf16[256,2048]{1,0:T(8,128)(2,1)S(1)}, bf16[256,2048]{1,0:T(8,128)(2,1)}, u32[]{:S(2)}) copy-start(bf16[256,2048]{1,0:T(8,128)(2,1)} %param.10) | copy-start | bytes 3145732
  2.1 4.6 %copy-start.3 = (bf16[2048,64]{0,1:T(8,128)(2,1)S(1)}, bf16[2048,64]{0,1:T(8,128)(2,1)}, u32[]{:S(2)}) copy-start(bf16[2048,64]{0,1:T(8,128)(2,1)} %param.8) | copy-start | bytes 786436
  2.1 5.6 %copy-start.4 = (bf16[2048,64]{0,1:T(8,128)(2,1)S(1)}, bf16[2048,64]{0,1:T(8,128)(2,1)}, u32[]{:S(2)}) copy-start(bf16[2048,64]{0,1:T(8,128)(2,1)} %param.9) | copy-start | bytes 786436
  2.1 19.7 %all-to-all-start = ((bf16[4,64,2048]{2,1,0:T(8,128)(2,1)}), bf16[4,64,2048]{2,1,0:T(8,128)(2,1)S(1)}, u32[]{:S(2)}, u32[]{:S(2)}) async-start(bf16[4,64,2048]{2,1,0:T(8,128)(2,1)} %broadcast_in_dim.6), calls=%async_computation | async-start | bytes 2097152 | tf_op jit(solution)/shard_map/all_to_all | solution.py:195
  21.8 1.0 copy-start.1
  26.3 20.5 %copy-start.5 = (bf16[144,256]{1,0:T(8,128)(2,1)S(1)}, bf16[144,256]{1,0:T(8,128)(2,1)}, u32[]{:S(2)}) copy-start(bf16[144,256]{1,0:T(8,128)(2,1)} %get-tuple-element.14) | copy-start | bytes 221188
  27.2 14.4 %collective-permute-start = (bf16[256,128]{1,0:T(8,128)(2,1)S(1)}, bf16[256,128]{1,0:T(8,128)(2,1)S(1)}, u32[]{:S(2)}, u32[]{:S(2)}) collective-permute-start(bf16[256,128]{1,0:T(8,128)(2,1)S(1)} %get-tuple-element.22), channel_id=1, source_target_pairs={{0,480},{32,448},{64,416},{96,384},{128,352},{160,320},{192,288},{... | collective-permute-start | bytes 196616 | tf_op jit(solution)/shard_map/ppermute | solution.py:204
  42.5 44.0 %all-to-all-start.1 = ((bf16[4,2,256,128]{3,2,1,0:T(8,128)(2,1)}), bf16[4,2,256,128]{3,2,1,0:T(8,128)(2,1)S(1)}, u32[]{:S(2)}, u32[]{:S(2)}) async-start(bf16[4,2,256,128]{3,2,1,0:T(8,128)(2,1)} %broadcast_in_dim.7), calls=%async_computation.1 | async-start | bytes 1048576 | tf_op jit(solution)/shard_map/all_to_all | solution.py:195
  80.6 23.6 %collective-permute-start.1 = (bf16[8,144,256]{2,1,0:T(8,128)(2,1)S(1)}, bf16[8,144,256]{2,1,0:T(8,128)(2,1)S(1)}, u32[]{:S(2)}, u32[]{:S(2)}) collective-permute-start(bf16[8,144,256]{2,1,0:T(8,128)(2,1)S(1)} %bitcast.26), channel_id=1, source_target_pairs={{0,32},{32,0},{1,33},{33,1},{2,34},{34,2},{3,35},{35,3},{4,36},{36... | collective-permute-start | bytes 1769480 | tf_op jit(solution)/shard_map/ppermute | solution.py:206
  84.2 22.6 %collective-permute-start.3 = (bf16[8,144,256]{2,1,0:T(8,128)(2,1)S(1)}, bf16[8,144,256]{2,1,0:T(8,128)(2,1)S(1)}, u32[]{:S(2)}, u32[]{:S(2)}) collective-permute-start(bf16[8,144,256]{2,1,0:T(8,128)(2,1)S(1)} %bitcast.27), channel_id=1, source_target_pairs={{0,4},{4,0},{1,5},{5,1},{2,6},{6,2},{3,7},{7,3},{8,12},{12,8},{9,1... | collective-permute-start | bytes 1769480 | tf_op jit(solution)/shard_map/ppermute | solution.py:207
  104.2 35.7 %collective-permute-start.2 = (bf16[8,144,256]{2,1,0:T(8,128)(2,1)S(1)}, bf16[8,144,256]{2,1,0:T(8,128)(2,1)S(1)}, u32[]{:S(2)}, u32[]{:S(2)}) collective-permute-start(bf16[8,144,256]{2,1,0:T(8,128)(2,1)S(1)} %collective-permute-done.1.kv_ref), channel_id=1, source_target_pairs={{0,4},{4,0},{1,5},{5,1},{2,6},{6,2},{3,7},{7,3},{8,12},{12,8},{9,1... | collective-permute-start | bytes 1769480 | tf_op jit(solution)/shard_map/ppermute | solution.py:208
  172.8 5.5 %copy-start.2 = (bf16[2,256,128]{2,1,0:T(8,128)(2,1)S(1)}, bf16[2,256,128]{2,1,0:T(8,128)(2,1)}, u32[]{:S(2)}) copy-start(bf16[2,256,128]{2,1,0:T(8,128)(2,1)} %combine.1) | copy-start | bytes 393220
  174.8 15.6 %all-to-all-start.3 = ((bf16[4,32,2048]{2,1,0:T(8,128)(2,1)}), bf16[4,32,2048]{2,1,0:T(8,128)(2,1)S(1)}, u32[]{:S(2)}, u32[]{:S(2)}) async-start(bf16[4,32,2048]{2,1,0:T(8,128)(2,1)} %bitcast.16), calls=%async_computation.3 | async-start | bytes 1048576 | tf_op jit(solution)/shard_map/all_to_all | solution.py:230
  178.3 11.0 %collective-permute-start.4 = (bf16[256,128]{1,0:T(8,128)(2,1)S(1)}, bf16[256,128]{1,0:T(8,128)(2,1)S(1)}, u32[]{:S(2)}, u32[]{:S(2)}) collective-permute-start(bf16[256,128]{1,0:T(8,128)(2,1)S(1)} %slice_bitcast_fusion), channel_id=1, source_target_pairs={{0,480},{32,448},{64,416},{96,384},{128,352},{160,320},{192,288},{... | collective-permute-start | bytes 196616 | tf_op jit(solution)/shard_map/ppermute | solution.py:226
  190.5 12.8 %all-to-all-start.4 = ((bf16[4,32,2048]{2,1,0:T(8,128)(2,1)}), bf16[4,32,2048]{2,1,0:T(8,128)(2,1)S(1)}, u32[]{:S(2)}, u32[]{:S(2)}) async-start(bf16[4,32,2048]{2,1,0:T(8,128)(2,1)} %bitcast.18), calls=%async_computation.4 | async-start | bytes 1048576 | tf_op jit(solution)/shard_map/all_to_all | solution.py:230

commit v2 on v1

v2 whole, which is shorter than its diff:
```python
import functools
import math

import jax
import jax.numpy as jnp
from jax import lax
from jax.experimental import pallas as pl
from jax.experimental.pallas import tpu as pltpu
from jax.sharding import Mesh, PartitionSpec as P

HD = 64
ROWS = 256
HALF = 128
GROUP = 4
KROWS = 80
QROWS = 144
VROWS = 72
LOG2E = math.log2(math.e)
JUMP_LIMIT = 64.0
NEG_START = -1e30
NEG_MASKED = -2e30
BF = jnp.bfloat16
F32 = jnp.float32
SWAP = ((0, 1), (1, 0))
VMEM = pl.BlockSpec(memory_space=pltpu.VMEM)
SMEM = pl.BlockSpec(memory_space=pltpu.SMEM)


def three_parts(x):
    high = x.astype(BF)
    rest = x - high.astype(F32)
    middle = rest.astype(BF)
    low = (rest - middle.astype(F32)).astype(BF)
    return high, middle, low


def packed(x):
    return jnp.concatenate([*three_parts(x), jnp.zeros(x.shape, BF)], axis=0)


def project_kernel(x_ref, wq_ref, wk_ref, wv_ref, gate_ref, q_ref, kv_ref):
    x = x_ref[...].reshape(ROWS, x_ref.shape[2])
    across = (((1,), (1,)), ((), ()))
    query = jnp.dot(x, wq_ref[...], preferred_element_type=F32)
    key = lax.dot_general(x, wk_ref[...], across, preferred_element_type=F32)
    levels = gate_ref[...] * -LOG2E
    for part in range(2):
        starts = [y * 64 + part * 32 for y in range(4)]
        turned = jnp.concatenate([query[at : at + 32] for at in starts], axis=0).T.astype(BF)
        q_ref[part, 0:256] = turned
        keys = jnp.concatenate([key[at : at + 32] for at in starts], axis=0).T.astype(BF).astype(F32)
        own = turned.astype(F32).reshape(GROUP, HD, HALF) * keys
        level = jnp.concatenate([levels[:, at : at + 32] for at in starts], axis=1)
        q_ref[part, 256:272] = packed(jnp.sum(own, axis=1) * (LOG2E * 0.125) + level)
    kv_ref[0:64] = lax.dot_general(wk_ref[...], x, across, preferred_element_type=F32).astype(BF)
    kv_ref[KROWS : KROWS + 64] = lax.dot_general(wv_ref[...], x, across, preferred_element_type=F32).astype(BF)
    kv_ref[64:80] = packed(levels)


def project(x, w_query, w_key, w_value, gate):
    return pl.pallas_call(
        project_kernel,
        in_specs=[VMEM] * 5,
        out_specs=[VMEM] * 2,
        out_shape=[
            jax.ShapeDtypeStruct((2, GROUP * HD + 16, HALF), BF),
            jax.ShapeDtypeStruct((KROWS + 64, ROWS), BF),
        ],
        cost_estimate=pl.CostEstimate(flops=2 * 256 * 2048 * 384, bytes_accessed=3 << 20, transcendentals=0),
        name="project",
    )(x, w_query, w_key, w_value, gate)


def attend_kernel(first, last, sc_ref, q0_ref, q1_ref, q2_ref, q3_ref, own_ref, swapped_ref, *refs):
    q_refs = (q0_ref, q1_ref, q2_ref, q3_ref)
    if first:
        refs = list(refs)
    else:
        acc_in, top_in, *refs = refs
    if last:
        out_ref, acc, top, *refs = refs
    else:
        acc, top, *refs = refs
    qa, ks, vs, saved_acc, saved_top, jump = refs
    if first:
        acc[...] = jnp.zeros_like(acc)
        for part in range(2):
            for xq in range(4):
                rows = q_refs[xq][part, 256:272, :].astype(F32)
                sums = rows[0:4] + rows[4:8] + rows[8:12]
                for h in range(GROUP):
                    top[part, xq, :, h * HALF : (h + 1) * HALF] = sums[h : h + 1]
    else:
        acc[...] = acc_in[...]
        top[...] = top_in[...]
    row = lax.broadcasted_iota(jnp.int32, (16, 512), 0)
    head = lax.broadcasted_iota(jnp.int32, (16, 512), 1) // HALF
    chooser = jnp.where((row < 12) & (row % 4 == head), 1.0, 0.0).astype(BF)
    for part in range(2):
        for xq in range(4):
            for h in range(GROUP):
                cols = slice(h * HALF, (h + 1) * HALF)
                scaled = q_refs[xq][part, h * HD : (h + 1) * HD, :].astype(F32) * (LOG2E * 0.125)
                high = scaled.astype(BF)
                qa[part, xq, 0:64, cols] = high
                qa[part, xq, 64:128, cols] = (scaled - high.astype(F32)).astype(BF)
            qa[part, xq, 128:144, :] = chooser
    for b in range(8):
        for side, ref in enumerate((own_ref, swapped_ref)):
            keys = ref[b, 0:KROWS, :].astype(F32)
            at = slice((2 * b + side) * ROWS, (2 * b + side + 1) * ROWS)
            ks[at, 0:QROWS] = jnp.concatenate([keys[0:64], keys], axis=0).T.astype(BF)
            cols = slice(side * ROWS, (side + 1) * ROWS)
            vs[b, 0:64, cols] = ref[b, KROWS : KROWS + 64, :]
            vs[b, 64:72, cols] = jnp.ones((8, ROWS), BF)

    def masked(scores, part, xq, start):
        key = lax.broadcasted_iota(jnp.int32, scores.shape, 0)
        key_pos = key + jnp.where(key < ROWS, start + sc_ref[5], start - sc_ref[5])
        lane = lax.broadcasted_iota(jnp.int32, (1, scores.shape[1]), 1) % HALF
        query_pos = sc_ref[6 + xq] * 512 + sc_ref[5] + part * 32 + (lane // 32) * 64 + lane % 32
        return jnp.where(key_pos <= query_pos, scores, NEG_MASKED)

    def careful_step(part, plane, start):
        keys = ks[pl.ds(pl.multiple_of(plane * 512, 512), 512), 0:QROWS]
        tiles = [(xq, slice(side * 256, side * 256 + 256)) for xq in range(4) for side in range(2)]

        def score(i):
            xq, cols = tiles[i]
            scores = jnp.dot(keys, qa[part, xq, :, cols], preferred_element_type=F32)
            return scores if start is None else masked(scores, part, xq, start)

        def soften(i, scores):
            xq, cols = tiles[i]
            old = top[part, xq, :, cols]
            new = jnp.maximum(old, jnp.max(scores, axis=0, keepdims=True))
            top[part, xq, :, cols] = new
            return jnp.exp2(scores - new).astype(BF), jnp.exp2(old - new)

        def gather(i, weights, decay):
            xq, cols = tiles[i]
            update = jnp.dot(vs[plane], weights, preferred_element_type=F32)
            acc[part, xq, :, cols] = acc[part, xq, :, cols] * decay + update

        waiting = score(0)
        pending = None
        for i in range(8):
            following = score(i + 1) if i < 7 else None
            if pending is not None:
                gather(i - 1, *pending)
            pending = soften(i, waiting)
            waiting = following
        gather(7, *pending)

    def quick_step(part, plane, start):
        keys = ks[pl.ds(pl.multiple_of(plane * 512, 512), 512), 0:QROWS]

        def soften(xq):
            scores = jnp.dot(keys, qa[part, xq], preferred_element_type=F32)
            if start is not None:
                scores = masked(scores, part, xq, start)
            old = top[part, xq]
            weights = jnp.exp2(scores - old).astype(BF)
            largest = jnp.max(scores, axis=0, keepdims=True)
            new = jnp.maximum(old, largest)
            top[part, xq] = new
            jump[...] = jnp.maximum(jump[...], largest - old)
            return weights, jnp.exp2(old - new)

        def gather(xq, weights, decay):
            update = jnp.dot(vs[plane], weights, preferred_element_type=F32)
            acc[part, xq] = (acc[part, xq] + update) * decay

        pending = soften(0)
        for xq in range(4):
            following = soften(xq + 1) if xq < 3 else None
            gather(xq, *pending)
            pending = following

    def one_part(part, carry):
        full = sc_ref[part]
        end = full + sc_ref[2 + part]

        def over(step):
            def whole(i, c):
                step(part, i, None)
                return c

            def edge(i, c):
                step(part, i, sc_ref[4])
                return c

            lax.fori_loop(0, full, whole, 0)
            lax.fori_loop(full, end, edge, 0)

        saved_acc[...] = acc[part]
        saved_top[...] = top[part]
        jump[...] = jnp.zeros_like(jump)
        over(quick_step)

        @pl.when(jnp.max(jump[...]) > JUMP_LIMIT)
        def _():
            acc[part] = saved_acc[...]
            top[part] = saved_top[...]
            over(careful_step)

        return carry

    lax.fori_loop(0, 2, one_part, 0)
    if last:
        for part in range(2):
            for xq in range(4):
                total = acc[part, xq, 64:65, :]
                some = total > 0.0
                safe = jnp.where(some, total, 1.0)
                out_ref[sc_ref[6 + xq], part, 0:64] = (acc[part, xq, 0:64, :] / safe).astype(BF)
                level = jnp.where(some, top[part, xq] + jnp.log2(safe), NEG_START)
                high, middle, low = three_parts(level)
                out_ref[sc_ref[6 + xq], part, 64:72] = jnp.concatenate([high, middle, low, jnp.zeros((5, 512), BF)], axis=0)


def attend(scalars, queries, own, swapped, state, last):
    first = state is None
    args = [scalars, *queries, own, swapped] + ([] if first else list(state))
    acc_shape = (2, 4, VROWS, 512)
    top_shape = (2, 4, 1, 512)
    scratch = [
        pltpu.VMEM((2, 4, QROWS, 512), BF),
        pltpu.VMEM((16 * ROWS, 256), BF),
        pltpu.VMEM((8, VROWS, 512), BF),
        pltpu.VMEM(acc_shape[1:], F32),
        pltpu.VMEM(top_shape[1:], F32),
        pltpu.VMEM((1, 512), F32),
    ]
    if last:
        out_shape = [jax.ShapeDtypeStruct((4, 2, VROWS, 512), BF)]
        scratch = [pltpu.VMEM(acc_shape, F32), pltpu.VMEM(top_shape, F32)] + scratch
    else:
        out_shape = [jax.ShapeDtypeStruct(acc_shape, F32), jax.ShapeDtypeStruct(top_shape, F32)]
    return pl.pallas_call(
        functools.partial(attend_kernel, first, last),
        in_specs=[SMEM] + [VMEM] * (len(args) - 1),
        out_specs=[VMEM] * len(out_shape),
        out_shape=out_shape,
        scratch_shapes=scratch,
        cost_estimate=pl.CostEstimate(flops=10_000_000_000, bytes_accessed=4 << 20, transcendentals=8 << 20),
        compiler_params=pltpu.CompilerParams(vmem_limit_bytes=40 << 20),
        name="attend",
    )(*args)


def combine_kernel(x_ref, o_ref):
    for part in range(2):
        levels = []
        for s in range(4):
            high, middle, low = (x_ref[s, part, 64 + j : 65 + j, :].astype(F32) for j in range(3))
            levels.append(high + middle + low)
        top = jnp.maximum(jnp.maximum(levels[0], levels[1]), jnp.maximum(levels[2], levels[3]))
        shares = [jnp.exp2(level - top) for level in levels]
        total = shares[0] + shares[1] + shares[2] + shares[3]
        mixed = x_ref[0, part, 0:64, :].astype(F32) * shares[0]
        for s in range(1, 4):
            mixed += x_ref[s, part, 0:64, :].astype(F32) * shares[s]
        mixed = (mixed / total).astype(BF)
        for h in range(GROUP):
            o_ref[part, h * HD : (h + 1) * HD, :] = mixed[:, h * HALF : (h + 1) * HALF]


def combine(x):
    return pl.pallas_call(
        combine_kernel,
        in_specs=[VMEM],
        out_specs=VMEM,
        out_shape=jax.ShapeDtypeStruct((2, GROUP * HD, HALF), BF),
        cost_estimate=pl.CostEstimate(flops=1_000_000, bytes_accessed=1 << 20, transcendentals=0),
        name="combine",
    )(x)


def sent_to_all(x, axis):
    copies = jnp.broadcast_to(x, (lax.axis_size(axis), *x.shape))
    return lax.all_to_all(copies, axis, split_axis=0, concat_axis=0, tiled=True)


def per_device(tokens, w_query, w_key, w_value, w_out, cum_gate):
    zh, zl, x, c = (lax.axis_index(a) for a in ("zh", "zl", "x", "c"))
    plane = zh * 2 + zl
    mirror = [(i, 15 - i) for i in range(16)]
    rows = sent_to_all(tokens, "y")
    queries, kv = project(rows, w_query, w_key.T, w_value.T, cum_gate)
    same_own = sent_to_all(kv, "zh")
    moved = lax.ppermute(queries[1], ("zh", "zl"), mirror)
    ours = jnp.stack([queries[0], moved])
    gathered = [ours] + [lax.ppermute(ours, "x", [(i, (i + j) % 4) for i in range(4)]) for j in (2, 1, 3)]
    gathered = [gathered[0], gathered[2], gathered[1], gathered[3]]
    same_own, gathered = lax.optimization_barrier((same_own, gathered))
    other_own = lax.ppermute(same_own, "zl", SWAP)
    same_swapped = lax.ppermute(same_own, "c", SWAP)
    state = None
    for number in range(2):
        parity = zl if number == 0 else 1 - zl
        scalars = jnp.stack(
            [
                (plane - parity + 1) // 2,
                (15 - plane - parity + 1) // 2,
                1 - (plane - parity) % 2,
                1 - (15 - plane - parity) % 2,
                x * 512,
                c * ROWS,
                *((x - j) % 4 for j in range(4)),
            ]
        ).astype(jnp.int32)
        if number == 0:
            state = attend(scalars, gathered, same_own, same_swapped, state, False)
        else:
            level, other_own = lax.optimization_barrier((state[1], other_own))
            state = (state[0], level)
            other_swapped = lax.ppermute(other_own, "c", SWAP)
            state = attend(scalars, gathered, other_own, other_swapped, state, True)
    shared = lax.all_to_all(state[0], "x", 0, 0, tiled=True)
    mixed = combine(shared)
    back = lax.ppermute(mixed[1], ("zh", "zl"), mirror)
    outs = []
    for half in (mixed[0], back):
        share = lax.dot_general(half, w_out, (((0,), (0,)), ((), ())), preferred_element_type=F32).astype(BF)
        pieces = lax.all_to_all(share.reshape(4, 32, -1), "y", 0, 0, tiled=True)
        outs.append(jnp.sum(pieces.astype(F32), axis=0).astype(BF))
    return jnp.concatenate(outs, axis=0)


def solution(mesh):
    fine = Mesh(mesh.devices.reshape(8, 2, 4, 2, 4), ("zh", "zl", "x", "c", "y"))
    sp = ("zh", "zl", "x", "c")
    placed = (
        P((*sp, "y"), None),
        P(None, "y"),
        P(None, "y"),
        P(None, "y"),
        P("y", None),
        P("y", sp),
    )
    return jax.shard_map(per_device, mesh=fine, in_specs=placed, out_specs=P((*sp, "y"), None), check_vma=False)
```

time: 205 us -> 189 us (0.922)
  the two profiles are of different devices: /device:TPU:64 before, /device:TPU:96 now
where the time goes in v2:
time: 189 us; the launch traced here: 192 us
  starting transfers between devices  65.1 us (34%)
  waiting for transfers between devices  42.7 us (23%)
  blocking collectives  37 us (20%)
  Pallas kernels  36.9 us (20%)
  local copies, waits for them, and re-layouts  5.42 us (3%)
  matrix products  3.17 us (2%)
    pallas_call x2, Pallas kernels, attend(): pl.pallas_call(functools.partial(attend_kernel, first, last), in_specs=[S...  31.5 us
    all_to_all x1, blocking collectives, sent_to_all(): return lax.all_to_all(copies, axis, split_axis=0, concat_axis=0, tiled=True)  19.5 us
    ppermute x1, waiting for transfers between devices, per_device(): moved = lax.ppermute(queries[1], ('zh', 'zl'), mirror)  19.2 us
    all_to_all x2, starting transfers between devices, per_device(): pieces = lax.all_to_all(share.reshape(4, 32, -1), 'y', 0, 0, tiled=True)  18 us
    all_to_all x1, blocking collectives, per_device(): shared = lax.all_to_all(state[0], 'x', 0, 0, tiled=True)  17.6 us
    all_to_all x1, starting transfers between devices, sent_to_all(): return lax.all_to_all(copies, axis, split_axis=0, concat_axis=0, tiled=True)  13.8 us
    ppermute x3, starting transfers between devices, per_device(): lax.ppermute(ours, 'x', [(i, (i + j) % 4) for i in range(4)])  11.4 us
    ppermute x1, waiting for transfers between devices, per_device(): back = lax.ppermute(mixed[1], ('zh', 'zl'), mirror)  10.5 us
  transfers between devices with their start and end apart: 11, of which 6 were waited for; matrix products, arithmetic and copies ran while one was open for 1% of the time, Pallas kernels for 10%

profile of v2, /device:TPU:96, one launch (start us, length us, event | category | flops | bytes accessed | tf_op | source)
XLA Modules:
  0.0 191.5 jit_solution(9054626417688695662)
XLA Ops:
  0.0 0.0 copy-start
  0.0 1.1 broadcast_in_dim.6
  1.2 19.5 %all_to_all.25.x_ref = bf16[4,64,2048]{2,1,0:T(8,128)(2,1)} all-to-all(bf16[4,64,2048]{2,1,0:T(8,128)(2,1)S(1)} %broadcast_in_dim.6), channel_id=1, replica_groups=mesh['zh'=8,'zl'=2,'x'=4,'c'=2,'y'=4] {'y'}, dimensions={0} | all-to-all | bytes 2097152 | tf_op jit(solution)/shard_map/all_to_all | solution.py:282
  20.6 3.5 %project.1 = (bf16[2,272,128]{2,1,0:T(8,128)(2,1)}, bf16[144,256]{1,0:T(8,128)(2,1)}) custom-call(bf16[4,64,2048]{2,1,0:T(8,128)(2,1)} %all_to_all.25.x_ref, bf16[2048,256]{1,0:T(8,128)(2,1)} %wq_ref.1, bf16[64,2048]{1,0:T(8,128)(2,1)} %bitcast.29, bf16[64,2048]{1,0:T(8,128)(2,1)} %bitcast.30, f32[4,256]{1,0:T(4,128)} %gate_ref.1), custom_call_target="tpu_custom_call" | custom-call | flops 402653184 | bytes 3145728 | tf_op jit(solution)/shard_map/project/pallas_call | solution.py:61
  24.1 0.0 copy-start.4
  24.1 1.8 broadcast_in_dim.7
  25.9 13.8 %all-to-all-start.1 = ((bf16[8,144,256]{2,1,0:T(8,128)(2,1)}), bf16[8,144,256]{2,1,0:T(8,128)(2,1)S(1)}, u32[]{:S(2)}, u32[]{:S(2)}) async-start(bf16[8,144,256]{2,1,0:T(8,128)(2,1)} %broadcast_in_dim.7), calls=%async_computation.1 | async-start | bytes 1179648 | tf_op jit(solution)/shard_map/all_to_all | solution.py:282
  39.7 0.0 copy-done.4
  39.8 7.7 %collective-permute-start = (bf16[272,128]{1,0:T(8,128)(2,1)S(1)}, bf16[272,128]{1,0:T(8,128)(2,1)S(1)}, u32[]{:S(2)}, u32[]{:S(2)}) collective-permute-start(bf16[272,128]{1,0:T(8,128)(2,1)S(1)} %get-tuple-element.28), channel_id=1, source_target_pairs={{0,480},{32,448},{64,416},{96,384},{128,352},{160,320},{192,288},{... | collective-permute-start | bytes 208904 | tf_op jit(solution)/shard_map/ppermute | solution.py:292
  47.5 19.2 %collective-permute-done = bf16[272,128]{1,0:T(8,128)(2,1)S(1)} collective-permute-done((bf16[272,128]{1,0:T(8,128)(2,1)S(1)}, bf16[272,128]{1,0:T(8,128)(2,1)S(1)}, u32[]{:S(2)}, u32[]{:S(2)}) %collective-permute-start) | collective-permute-done | bytes 69664 | tf_op jit(solution)/shard_map/ppermute | solution.py:292
  66.8 3.4 %collective-permute-start.1 = (bf16[2,272,128]{2,1,0:T(8,128)(2,1)S(1)}, bf16[2,272,128]{2,1,0:T(8,128)(2,1)S(1)}, u32[]{:S(2)}, u32[]{:S(2)}) collective-permute-start(bf16[2,272,128]{2,1,0:T(8,128)(2,1)S(1)} %pad_maximum_fusion.1.q0_ref), channel_id=1, source_target_pairs={{0,8},{8,16},{16,24},{24,0},{1,9},{9,17},{17,25},{25,1},{2,10},{10... | collective-permute-start | bytes 417800 | tf_op jit(solution)/shard_map/ppermute | solution.py:294
  70.2 4.6 %collective-permute-start.2 = (bf16[2,272,128]{2,1,0:T(8,128)(2,1)S(1)}, bf16[2,272,128]{2,1,0:T(8,128)(2,1)S(1)}, u32[]{:S(2)}, u32[]{:S(2)}) collective-permute-start(bf16[2,272,128]{2,1,0:T(8,128)(2,1)S(1)} %pad_maximum_fusion.1.q0_ref), channel_id=1, source_target_pairs={{0,16},{8,24},{16,0},{24,8},{1,17},{9,25},{17,1},{25,9},{2,18},{10... | collective-permute-start | bytes 417800 | tf_op jit(solution)/shard_map/ppermute | solution.py:294
  74.8 3.3 %collective-permute-start.3 = (bf16[2,272,128]{2,1,0:T(8,128)(2,1)S(1)}, bf16[2,272,128]{2,1,0:T(8,128)(2,1)S(1)}, u32[]{:S(2)}, u32[]{:S(2)}) collective-permute-start(bf16[2,272,128]{2,1,0:T(8,128)(2,1)S(1)} %pad_maximum_fusion.1.q0_ref), channel_id=1, source_target_pairs={{0,24},{8,0},{16,8},{24,16},{1,25},{9,1},{17,9},{25,17},{2,26},{10... | collective-permute-start | bytes 417800 | tf_op jit(solution)/shard_map/ppermute | solution.py:294
  78.1 0.0 collective-permute-done.1.q1_ref
  78.1 0.5 collective-permute-done.2.q2_ref
  78.6 3.1 %collective-permute-done.3.q3_ref = bf16[2,272,128]{2,1,0:T(8,128)(2,1)S(1)} collective-permute-done((bf16[2,272,128]{2,1,0:T(8,128)(2,1)S(1)}, bf16[2,272,128]{2,1,0:T(8,128)(2,1)S(1)}, u32[]{:S(2)}, u32[]{:S(2)}) %collective-permute-start.3) | collective-permute-done | bytes 139296 | tf_op jit(solution)/shard_map/ppermute | solution.py:294
  81.7 0.0 all-to-all-done.1.own_ref
  81.7 1.9 collective-permute-start.4
  83.8 0.1 stack.77.sc_ref
  83.8 7.6 %collective-permute-start.5 = (bf16[8,144,256]{2,1,0:T(8,128)(2,1)S(1)}, bf16[8,144,256]{2,1,0:T(8,128)(2,1)S(1)}, u32[]{:S(2)}, u32[]{:S(2)}) collective-permute-start(bf16[8,144,256]{2,1,0:T(8,128)(2,1)S(1)} %all-to-all-done.1.own_ref), channel_id=1, source_target_pairs={{0,32},{32,0},{1,33},{33,1},{2,34},{34,2},{3,35},{35,3},{4,36},{36... | collective-permute-start | bytes 1769480 | tf_op jit(solution)/shard_map/ppermute | solution.py:297
  91.5 0.0 collective-permute-done.4.swapped_ref
  91.5 19.9 %attend.2 = (f32[2,4,72,512]{3,2,1,0:T(8,128)S(1)}, f32[2,4,1,512]{3,2,1,0:T(1,128)S(1)}) custom-call(s32[10]{0:T(128)S(1)} %stack.77.sc_ref, bf16[2,272,128]{2,1,0:T(8,128)(2,1)S(1)} %pad_maximum_fusion.1.q0_ref, bf16[2,272,128]{2,1,0:T(8,128)(2,1)S(1)} %collective-permute-done.1.q1_ref, bf16[2,272,128]{2,1,0:T(8,128)(2,1)S(1)} %collective-permute-done.2.q2_ref, ...), custom_call_target="tpu_custom_call" | custom-call | flops 10000000000 | bytes 4194304 | tf_op jit(solution)/shard_map/attend/pallas_call | solution.py:240
  111.4 0.0 copy-start.1
  111.4 1.0 copy-done.1
  112.4 0.0 collective-permute-done.5.own_ref
  112.4 2.3 %collective-permute-start.6 = (bf16[8,144,256]{2,1,0:T(8,128)(2,1)S(1)}, bf16[8,144,256]{2,1,0:T(8,128)(2,1)S(1)}, u32[]{:S(2)}, u32[]{:S(2)}) collective-permute-start(bf16[8,144,256]{2,1,0:T(8,128)(2,1)S(1)} %collective-permute-done.5.own_ref), channel_id=1, source_target_pairs={{0,4},{4,0},{1,5},{5,1},{2,6},{6,2},{3,7},{7,3},{8,12},{12,8},{9,1... | collective-permute-start | bytes 1769480 | tf_op jit(solution)/shard_map/ppermute | solution.py:318
  114.8 0.1 stack.70.sc_ref
  114.9 1.4 collective-permute-done.6.swapped_ref
  116.3 0.0 copy-start.2
  116.3 1.3 copy-done.2
  117.6 11.6 %attend.3 = bf16[4,2,72,512]{3,2,1,0:T(8,128)(2,1)S(1)} custom-call(s32[10]{0:T(128)S(1)} %stack.70.sc_ref, bf16[2,272,128]{2,1,0:T(8,128)(2,1)S(1)} %pad_maximum_fusion.1.q0_ref, bf16[2,272,128]{2,1,0:T(8,128)(2,1)S(1)} %collective-permute-done.1.q1_ref, bf16[2,272,128]{2,1,0:T(8,128)(2,1)S(1)} %collective-permute-done.2.q2_ref, ...), custom_call_target="tpu_custom_call" | custom-call | flops 10000000000 | bytes 4194304 | tf_op jit(solution)/shard_map/attend/pallas_call | solution.py:240
  129.2 17.6 %all_to_all.26.x_ref = bf16[4,2,72,512]{3,2,1,0:T(8,128)(2,1)} all-to-all(bf16[4,2,72,512]{3,2,1,0:T(8,128)(2,1)S(1)} %attend.3), channel_id=1, replica_groups=mesh['zh'=8,'zl'=2,'x'=4,'c'=2,'y'=4] {'x'}, dimensions={0} | all-to-all | bytes 1179648 | tf_op jit(solution)/shard_map/all_to_all | solution.py:320
  146.7 1.9 combine.1
  148.6 0.0 copy-done
  148.6 0.0 copy-start.3
  148.6 2.0 %convolution_convert_fusion.1 = bf16[128,2048]{1,0:T(8,128)(2,1)} fusion(bf16[256,2048]{1,0:T(8,128)(2,1)S(1)} %copy-done, bf16[2,256,128]{2,1,0:T(8,128)(2,1)} %combine.1), kind=kOutput, calls=%fused_computation.1 | convolution fusion | flops 134479872 | bytes 1638400 | tf_op jit(solution)/shard_map/dot_general | solution.py:325
  150.7 13.2 %all-to-all-start.3 = ((bf16[4,32,2048]{2,1,0:T(8,128)(2,1)}), bf16[4,32,2048]{2,1,0:T(8,128)(2,1)S(1)}, u32[]{:S(2)}, u32[]{:S(2)}) async-start(bf16[4,32,2048]{2,1,0:T(8,128)(2,1)} %bitcast.19), calls=%async_computation.3 | async-start | bytes 1048576 | tf_op jit(solution)/shard_map/all_to_all | solution.py:326
  163.9 0.0 copy-done.3
  163.9 2.3 %collective-permute-start.7 = (bf16[256,128]{1,0:T(8,128)(2,1)S(1)}, bf16[256,128]{1,0:T(8,128)(2,1)S(1)}, u32[]{:S(2)}, u32[]{:S(2)}) collective-permute-start(bf16[256,128]{1,0:T(8,128)(2,1)S(1)} %slice_bitcast_fusion.1), channel_id=1, source_target_pairs={{0,480},{32,448},{64,416},{96,384},{128,352},{160,320},{192,288},{... | collective-permute-start | bytes 196616 | tf_op jit(solution)/shard_map/ppermute | solution.py:322
  166.2 10.5 %collective-permute-done.7 = bf16[256,128]{1,0:T(8,128)(2,1)S(1)} collective-permute-done((bf16[256,128]{1,0:T(8,128)(2,1)S(1)}, bf16[256,128]{1,0:T(8,128)(2,1)S(1)}, u32[]{:S(2)}, u32[]{:S(2)}) %collective-permute-start.7) | collective-permute-done | bytes 65568 | tf_op jit(solution)/shard_map/ppermute | solution.py:322
  176.7 1.1 convolution_convert_fusion
  177.8 0.0 all-to-all-done.3
  177.8 4.8 %all-to-all-start.4 = ((bf16[4,32,2048]{2,1,0:T(8,128)(2,1)}), bf16[4,32,2048]{2,1,0:T(8,128)(2,1)S(1)}, u32[]{:S(2)}, u32[]{:S(2)}) async-start(bf16[4,32,2048]{2,1,0:T(8,128)(2,1)} %bitcast.21), calls=%async_computation.4 | async-start | bytes 1048576 | tf_op jit(solution)/shard_map/all_to_all | solution.py:326
  182.6 0.1 reduce_sum.24
  182.7 8.0 %all-to-all-done.4 = bf16[4,32,2048]{2,1,0:T(8,128)(2,1)S(1)} async-done(((bf16[4,32,2048]{2,1,0:T(8,128)(2,1)}), bf16[4,32,2048]{2,1,0:T(8,128)(2,1)S(1)}, u32[]{:S(2)}, u32[]{:S(2)}) %all-to-all-start.4) | async-done | bytes 524320 | tf_op jit(solution)/shard_map/all_to_all | solution.py:326
  190.7 0.1 reduce_sum.25
  190.8 0.7 pad_maximum_fusion
  (3 shorter events, 0.0 us)
Async XLA Ops:
  0.0 148.6 %copy-start = (bf16[256,2048]{1,0:T(8,128)(2,1)S(1)}, bf16[256,2048]{1,0:T(8,128)(2,1)}, u32[]{:S(2)}) copy-start(bf16[256,2048]{1,0:T(8,128)(2,1)} %param.10) | copy-start | bytes 3145732
  24.1 15.6 %copy-start.4 = (bf16[2,272,128]{2,1,0:T(8,128)(2,1)S(1)}, bf16[2,272,128]{2,1,0:T(8,128)(2,1)}, u32[]{:S(2)}) copy-start(bf16[2,272,128]{2,1,0:T(8,128)(2,1)} %get-tuple-element.17) | copy-start | bytes 417796
  25.9 55.8 %all-to-all-start.1 = ((bf16[8,144,256]{2,1,0:T(8,128)(2,1)}), bf16[8,144,256]{2,1,0:T(8,128)(2,1)S(1)}, u32[]{:S(2)}, u32[]{:S(2)}) async-start(bf16[8,144,256]{2,1,0:T(8,128)(2,1)} %broadcast_in_dim.7), calls=%async_computation.1 | async-start | bytes 1179648 | tf_op jit(solution)/shard_map/all_to_all | solution.py:282
  39.8 27.0 %collective-permute-start = (bf16[272,128]{1,0:T(8,128)(2,1)S(1)}, bf16[272,128]{1,0:T(8,128)(2,1)S(1)}, u32[]{:S(2)}, u32[]{:S(2)}) collective-permute-start(bf16[272,128]{1,0:T(8,128)(2,1)S(1)} %get-tuple-element.28), channel_id=1, source_target_pairs={{0,480},{32,448},{64,416},{96,384},{128,352},{160,320},{192,288},{... | collective-permute-start | bytes 208904 | tf_op jit(solution)/shard_map/ppermute | solution.py:292
  66.8 11.4 %collective-permute-start.1 = (bf16[2,272,128]{2,1,0:T(8,128)(2,1)S(1)}, bf16[2,272,128]{2,1,0:T(8,128)(2,1)S(1)}, u32[]{:S(2)}, u32[]{:S(2)}) collective-permute-start(bf16[2,272,128]{2,1,0:T(8,128)(2,1)S(1)} %pad_maximum_fusion.1.q0_ref), channel_id=1, source_target_pairs={{0,8},{8,16},{16,24},{24,0},{1,9},{9,17},{17,25},{25,1},{2,10},{10... | collective-permute-start | bytes 417800 | tf_op jit(solution)/shard_map/ppermute | solution.py:294
  70.2 8.5 %collective-permute-start.2 = (bf16[2,272,128]{2,1,0:T(8,128)(2,1)S(1)}, bf16[2,272,128]{2,1,0:T(8,128)(2,1)S(1)}, u32[]{:S(2)}, u32[]{:S(2)}) collective-permute-start(bf16[2,272,128]{2,1,0:T(8,128)(2,1)S(1)} %pad_maximum_fusion.1.q0_ref), channel_id=1, source_target_pairs={{0,16},{8,24},{16,0},{24,8},{1,17},{9,25},{17,1},{25,9},{2,18},{10... | collective-permute-start | bytes 417800 | tf_op jit(solution)/shard_map/ppermute | solution.py:294
  74.8 6.9 %collective-permute-start.3 = (bf16[2,272,128]{2,1,0:T(8,128)(2,1)S(1)}, bf16[2,272,128]{2,1,0:T(8,128)(2,1)S(1)}, u32[]{:S(2)}, u32[]{:S(2)}) collective-permute-start(bf16[2,272,128]{2,1,0:T(8,128)(2,1)S(1)} %pad_maximum_fusion.1.q0_ref), channel_id=1, source_target_pairs={{0,24},{8,0},{16,8},{24,16},{1,25},{9,1},{17,9},{25,17},{2,26},{10... | collective-permute-start | bytes 417800 | tf_op jit(solution)/shard_map/ppermute | solution.py:294
  81.7 9.7 %collective-permute-start.4 = (bf16[8,144,256]{2,1,0:T(8,128)(2,1)S(1)}, bf16[8,144,256]{2,1,0:T(8,128)(2,1)S(1)}, u32[]{:S(2)}, u32[]{:S(2)}) collective-permute-start(bf16[8,144,256]{2,1,0:T(8,128)(2,1)S(1)} %all-to-all-done.1.own_ref), channel_id=1, source_target_pairs={{0,4},{4,0},{1,5},{5,1},{2,6},{6,2},{3,7},{7,3},{8,12},{12,8},{9,1... | collective-permute-start | bytes 1769480 | tf_op jit(solution)/shard_map/ppermute | solution.py:298
  83.8 28.6 %collective-permute-start.5 = (bf16[8,144,256]{2,1,0:T(8,128)(2,1)S(1)}, bf16[8,144,256]{2,1,0:T(8,128)(2,1)S(1)}, u32[]{:S(2)}, u32[]{:S(2)}) collective-permute-start(bf16[8,144,256]{2,1,0:T(8,128)(2,1)S(1)} %all-to-all-done.1.own_ref), channel_id=1, source_target_pairs={{0,32},{32,0},{1,33},{33,1},{2,34},{34,2},{3,35},{35,3},{4,36},{36... | collective-permute-start | bytes 1769480 | tf_op jit(solution)/shard_map/ppermute | solution.py:297
  111.4 1.0 copy-start.1
  112.4 3.9 %collective-permute-start.6 = (bf16[8,144,256]{2,1,0:T(8,128)(2,1)S(1)}, bf16[8,144,256]{2,1,0:T(8,128)(2,1)S(1)}, u32[]{:S(2)}, u32[]{:S(2)}) collective-permute-start(bf16[8,144,256]{2,1,0:T(8,128)(2,1)S(1)} %collective-permute-done.5.own_ref), channel_id=1, source_target_pairs={{0,4},{4,0},{1,5},{5,1},{2,6},{6,2},{3,7},{7,3},{8,12},{12,8},{9,1... | collective-permute-start | bytes 1769480 | tf_op jit(solution)/shard_map/ppermute | solution.py:318
  116.3 1.3 copy-start.2
  148.6 15.3 %copy-start.3 = (bf16[2,256,128]{2,1,0:T(8,128)(2,1)S(1)}, bf16[2,256,128]{2,1,0:T(8,128)(2,1)}, u32[]{:S(2)}) copy-start(bf16[2,256,128]{2,1,0:T(8,128)(2,1)} %combine.1) | copy-start | bytes 393220
  150.7 27.1 %all-to-all-start.3 = ((bf16[4,32,2048]{2,1,0:T(8,128)(2,1)}), bf16[4,32,2048]{2,1,0:T(8,128)(2,1)S(1)}, u32[]{:S(2)}, u32[]{:S(2)}) async-start(bf16[4,32,2048]{2,1,0:T(8,128)(2,1)} %bitcast.19), calls=%async_computation.3 | async-start | bytes 1048576 | tf_op jit(solution)/shard_map/all_to_all | solution.py:326
  163.9 12.8 %collective-permute-start.7 = (bf16[256,128]{1,0:T(8,128)(2,1)S(1)}, bf16[256,128]{1,0:T(8,128)(2,1)S(1)}, u32[]{:S(2)}, u32[]{:S(2)}) collective-permute-start(bf16[256,128]{1,0:T(8,128)(2,1)S(1)} %slice_bitcast_fusion.1), channel_id=1, source_target_pairs={{0,480},{32,448},{64,416},{96,384},{128,352},{160,320},{192,288},{... | collective-permute-start | bytes 196616 | tf_op jit(solution)/shard_map/ppermute | solution.py:322
  177.8 12.9 %all-to-all-start.4 = ((bf16[4,32,2048]{2,1,0:T(8,128)(2,1)}), bf16[4,32,2048]{2,1,0:T(8,128)(2,1)S(1)}, u32[]{:S(2)}, u32[]{:S(2)}) async-start(bf16[4,32,2048]{2,1,0:T(8,128)(2,1)} %bitcast.21), calls=%async_computation.4 | async-start | bytes 1048576 | tf_op jit(solution)/shard_map/all_to_all | solution.py:326
